TPU v7x, 32 devices: a whole 2x2x4 slice. The times are simulated.
32 devices in a mesh: grp: 2 (over x), tp: 4 (over z), dp: 4 (over y, core).
Axes of the slice: x: 2, y: 2, z: 4, core: 2. Of those that a mesh axis runs over, the one named last changes fastest.
Arguments:
- hidden: bfloat16 [16, 2048], P('grp', 'dp'), parts along dimension 0, may hold values from -20 to 20
- lengths: int32 [16], P(('grp', 'dp')), parts along dimension 0, may hold values from 1 to 256, 512 in all
- input_norm_gain: float32 [2, 2048], P(None, 'dp'), may hold values from 0.1 to 1.9
- gate_matrix: bfloat16 [2, 2048, 4096], P(None, 'dp', 'tp'), may hold values from -0.125 to 0.125
- input_matrix: bfloat16 [2, 2048, 4096], P(None, 'dp', 'tp'), may hold values from -0.125 to 0.125
- write_matrix: bfloat16 [2, 2048, 2048], P(None, 'dp', 'tp'), may hold values from -0.125 to 0.125
- read_matrix: bfloat16 [2, 2048, 2048], P(None, 'dp', 'tp'), may hold values from -0.125 to 0.125
- step_matrix: bfloat16 [2, 2048, 64], P(None, 'dp'), may hold values from -0.125 to 0.125
- step_size_bias: float32 [2, 64], P(None, 'tp'), may hold values from -2 to 1
- log_decay_rate: float32 [2, 64], P(None, 'tp'), may hold values from -1 to 2
- direct_path_gain: float32 [2, 64], P(None, 'tp'), may hold values from 0.5 to 1.5
- input_filter_taps: bfloat16 [2, 4, 4096], P(None, None, 'tp'), may hold values from -3 to 3
- write_filter_taps: bfloat16 [2, 4, 2048], P(None, None, 'tp'), may hold values from -3 to 3
- read_filter_taps: bfloat16 [2, 4, 2048], P(None, None, 'tp'), may hold values from -3 to 3
- position_log_decay: float32 [2, 256, 64], P(None, None, 'tp'), may hold values from -0.7 to 0
- grouped_norm_gain: float32 [2, 4096], P(None, 'tp'), may hold values from 0.1 to 1.9
- output_matrix: bfloat16 [2, 4096, 2048], P(None, 'tp', 'dp'), may hold values from -0.09375 to 0.09375
- recurrent_head_state: float32 [2, 16, 64, 64, 128], P(None, ('grp', 'dp'), 'tp'), parts along dimension 1, may hold values from -3 to 3
- history_input_rows: bfloat16 [2, 16, 3, 4096], P(None, ('grp', 'dp'), None, 'tp'), parts along dimension 1, may hold values from -5 to 5
- history_write_rows: bfloat16 [2, 16, 3, 2048], P(None, ('grp', 'dp'), None, 'tp'), parts along dimension 1, may hold values from -5 to 5
- history_read_rows: bfloat16 [2, 16, 3, 2048], P(None, ('grp', 'dp'), None, 'tp'), parts along dimension 1, may hold values from -5 to 5
Outputs:
- stream_out: bfloat16 [16, 2048], P('grp', 'dp'), parts along dimension 0
- state_out: float32 [2, 16, 64, 64, 128], P(None, ('grp', 'dp'), 'tp'), parts along dimension 1
- buffer_value_out: bfloat16 [2, 16, 3, 4096], P(None, ('grp', 'dp'), None, 'tp'), parts along dimension 1
- buffer_write_out: bfloat16 [2, 16, 3, 2048], P(None, ('grp', 'dp'), None, 'tp'), parts along dimension 1
- buffer_read_out: bfloat16 [2, 16, 3, 2048], P(None, ('grp', 'dp'), None, 'tp'), parts along dimension 1
There are 2 independent parts, one for each index of `grp`. A program takes and returns all parts, laid end to end along the dimension named above; an argument that names none is the same for every part. Nothing has to cross between parts.
Inputs may be any that keep to these rules, and one draw needn't show every extreme that they name: `lengths`: a sequence's current token stands at position length - 1; some sequence has length 256.
All inputs are finite; a program needn't handle non-finite values. No bound on the sum of `lengths` on one device may be relied on, other than what follows from the above.
Results may differ from a plain program's by a relative error of at most 0.0065.
Values may be sent and summed in bfloat16 or wider, within the bound.
No kernel may reach another device: no remote copies, remote signals or barrier semaphores. Data moves between devices by JAX's collectives and lax.ppermute only.
A program may use at most 64 MiB of HBM per device.

v0:
```python
import jax
import jax.numpy as jnp
from jax import lax
from jax.sharding import PartitionSpec as P

D = 2048
epsilon = 1e-06


def convolve(buffer, new_row, weights, tap_valid):
    tap_rows = weights.astype(jnp.float32)
    depth = weights.shape[0] - 1
    summed = new_row.astype(jnp.float32) * tap_rows[depth]
    for k in range(depth):
        summed = summed + buffer[:, k].astype(jnp.float32) * tap_rows[k] * tap_valid[:, k : k + 1]
    shifted = jnp.concatenate([buffer[:, 1:], new_row[:, None]], axis=1)
    return (jax.nn.silu(summed), shifted)


def spread_groups(rows, seq_local, groups_local, per_group, state_dim):
    grouped = rows.reshape(seq_local, groups_local, 1, state_dim)
    return jnp.broadcast_to(grouped, (seq_local, groups_local, per_group, state_dim)).reshape(
        seq_local, groups_local * per_group, state_dim
    )


def on_device(
    hidden,
    lengths,
    input_norm_gain,
    gate_matrix,
    input_matrix,
    write_matrix,
    read_matrix,
    step_matrix,
    step_size_bias,
    log_decay_rate,
    direct_path_gain,
    input_filter_taps,
    write_filter_taps,
    read_filter_taps,
    position_log_decay,
    grouped_norm_gain,
    output_matrix,
    recurrent_head_state,
    history_input_rows,
    history_write_rows,
    history_read_rows,
):
    seq_local = lengths.shape[0]
    heads_local = step_size_bias.shape[1]
    head_dim = recurrent_head_state.shape[3]
    state_dim = recurrent_head_state.shape[4]
    groups_local = write_filter_taps.shape[2] // state_dim
    per_group = heads_local // groups_local
    inner_local = heads_local * head_dim
    shared_local = groups_local * state_dim
    depth = input_filter_taps.shape[1] - 1
    token_position = lengths - 1
    tap_valid = (jnp.arange(depth)[None, :] >= depth - token_position[:, None]).astype(jnp.float32)
    state_is_valid = (token_position > 0).astype(jnp.float32)[:, None]
    position_indicator = (
        token_position[:, None] == jnp.arange(position_log_decay.shape[1])[None, :]
    ).astype(jnp.float32)
    head_first = lax.axis_index("tp") * heads_local
    seq_first = lax.axis_index("dp") * seq_local
    share_rows = hidden.shape[0] // lax.axis_size("tp")
    share_first = lax.axis_index("tp") * share_rows
    stream = hidden
    states, values, writes, reads = ([], [], [], [])
    for layer_index in range(input_norm_gain.shape[0]):
        stream_float = stream.astype(jnp.float32)
        squares = jnp.sum(stream_float * stream_float, axis=1)
        normed = (stream_float * input_norm_gain[layer_index]).astype(jnp.bfloat16)
        pieces = [
            jnp.dot(normed, weight[layer_index], preferred_element_type=jnp.float32)
            for weight in (gate_matrix, input_matrix, write_matrix, read_matrix)
        ]
        joined = jnp.concatenate(pieces, axis=1)
        step_weight = step_matrix[layer_index]
        step_term = jnp.dot(normed, step_weight, preferred_element_type=jnp.float32)
        squares_all = lax.psum(squares, "dp")
        joined_mine, step_mine = (
            lax.psum_scatter(joined, "dp", scatter_dimension=0, tiled=True),
            lax.psum_scatter(step_term, "dp", scatter_dimension=0, tiled=True),
        )
        mean_square = lax.dynamic_slice_in_dim(squares_all, seq_first, seq_local, 0) / D
        row_scale = lax.rsqrt(mean_square + epsilon)[:, None]
        step_raw = lax.dynamic_slice_in_dim(step_mine, head_first, heads_local, 1) * row_scale
        scaled = joined_mine * row_scale
        proj_gate = scaled[:, :inner_local]
        value_row = scaled[:, inner_local : 2 * inner_local].astype(jnp.bfloat16)
        write_row = scaled[:, 2 * inner_local : 2 * inner_local + shared_local].astype(jnp.bfloat16)
        read_row = scaled[:, 2 * inner_local + shared_local :].astype(jnp.bfloat16)
        value_act, value_buf = convolve(
            history_input_rows[layer_index], value_row, input_filter_taps[layer_index], tap_valid
        )
        write_act, write_buf = convolve(
            history_write_rows[layer_index], write_row, write_filter_taps[layer_index], tap_valid
        )
        read_act, read_buf = convolve(
            history_read_rows[layer_index], read_row, read_filter_taps[layer_index], tap_valid
        )
        head_step_size = jax.nn.softplus(step_raw + step_size_bias[layer_index])
        current_log_decay = jnp.dot(
            position_indicator, position_log_decay[layer_index], precision=lax.Precision.HIGHEST
        )
        current_decay = (
            jnp.exp(-jnp.exp(log_decay_rate[layer_index]) * head_step_size + current_log_decay)
            * state_is_valid
        )
        value_heads = value_act.reshape(seq_local, heads_local, head_dim)
        write_heads = spread_groups(write_act, seq_local, groups_local, per_group, state_dim)
        read_heads = spread_groups(read_act, seq_local, groups_local, per_group, state_dim)
        updated = (
            current_decay[:, :, None, None] * recurrent_head_state[layer_index]
            + (head_step_size[:, :, None] * value_heads)[:, :, :, None] * write_heads[:, :, None, :]
        )
        readout = jnp.einsum("shpn,shn->shp", updated, read_heads, precision=lax.Precision.HIGHEST)
        mixed_heads = (
            readout + direct_path_gain[layer_index][None, :, None] * value_heads
        ) * jax.nn.silu(proj_gate.reshape(seq_local, heads_local, head_dim))
        grouped = mixed_heads.reshape(seq_local, groups_local, per_group * head_dim)
        grouped = grouped * lax.rsqrt(jnp.mean(grouped * grouped, axis=2, keepdims=True) + epsilon)
        gated_rows = (
            grouped.reshape(seq_local, inner_local) * grouped_norm_gain[layer_index]
        ).astype(jnp.bfloat16)
        out_weight = output_matrix[layer_index]

        def project(rows_in, first_row, out_weight=out_weight):
            return jnp.dot(rows_in, out_weight, preferred_element_type=jnp.float32)

        partial_out = project(lax.all_gather(gated_rows, "dp", axis=0, tiled=True), jnp.int32(0))
        branch_share = lax.psum_scatter(partial_out, "tp", scatter_dimension=0, tiled=True)
        stream_share = lax.dynamic_slice_in_dim(stream_float, share_first, share_rows, 0)
        new_share = (stream_share + branch_share).astype(jnp.bfloat16)
        stream = lax.all_gather(new_share, "tp", axis=0, tiled=True)
        states.append(updated)
        values.append(value_buf)
        writes.append(write_buf)
        reads.append(read_buf)
    return (stream, jnp.stack(states), jnp.stack(values), jnp.stack(writes), jnp.stack(reads))


def solution(mesh):
    placed = (
        P("grp", "dp"),
        P(("grp", "dp")),
        P(None, "dp"),
        P(None, "dp", "tp"),
        P(None, "dp", "tp"),
        P(None, "dp", "tp"),
        P(None, "dp", "tp"),
        P(None, "dp", None),
        P(None, "tp"),
        P(None, "tp"),
        P(None, "tp"),
        P(None, None, "tp"),
        P(None, None, "tp"),
        P(None, None, "tp"),
        P(None, None, "tp"),
        P(None, "tp"),
        P(None, "tp", "dp"),
        P(None, ("grp", "dp"), "tp", None, None),
        P(None, ("grp", "dp"), None, "tp"),
        P(None, ("grp", "dp"), None, "tp"),
        P(None, ("grp", "dp"), None, "tp"),
    )
    return jax.shard_map(
        on_device,
        mesh=mesh,
        in_specs=placed,
        out_specs=(
            P("grp", "dp"),
            P(None, ("grp", "dp"), "tp", None, None),
            P(None, ("grp", "dp"), None, "tp"),
            P(None, ("grp", "dp"), None, "tp"),
            P(None, ("grp", "dp"), None, "tp"),
        ),
        check_vma=False,
    )
```

profile of v0, /device:TPU:0, one launch (start us, length us, event | category | flops | bytes accessed | tf_op | source)
XLA Modules:
  0.0 185.2 jit_solution(15273092470525130623)
XLA Ops:
  7.4 0.8 fusion.114
  8.2 1.3 fusion.38
  9.5 1.2 fusion.36
  10.8 1.5 fusion.17
  12.3 0.2 fusion.15
  12.5 0.7 pad_maximum_fusion.1
  13.3 0.1 multiply_reduce_fusion.3
  13.4 0.6 dynamic-slice
  14.7 0.5 slice_bitcast_fusion.31
  15.2 0.6 negate_bitcast_fusion
  15.8 0.1 fusion.52
  16.1 8.5 %all-reduce.7 = (f32[8]{0:T(128)S(1)}, f32[8,64]{1,0:T(8,128)S(1)}) all-reduce(f32[8]{0:T(128)S(1)} %multiply_reduce_fusion.3, f32[8,64]{1,0:T(8,128)S(1)} %fusion.52), channel_id=1, replica_groups=mesh['grp'=2,'tp'=4,'dp'=4] {'dp'}, use_global_device_ids=true, to_apply=%region_2.0 | all-reduce | flops 520 | bytes 4160 | tf_op jit(solution)/shard_map/psum | solution.py:82
  24.6 0.1 add_rsqrt_fusion.3
  24.7 0.6 fusion.111
  25.4 0.1 compare_select_fusion.1
  25.5 1.5 fusion.2
  27.0 0.6 slice_bitcast_fusion.30
  27.6 0.6 dynamic-slice.4
  28.8 19.0 %all-reduce.11.cloned.1.call-done = f32[8,3072]{1,0:T(8,128)} async-done(((f32[8,3072]{1,0:T(8,128)}), f32[8,3072]{1,0:T(8,128)}) %all-reduce.11.cloned.1.call-update) | async-done | bytes 98320
  47.8 1.0 fusion.106
  48.8 0.8 divide_multiply_fusion.5
  49.7 0.1 divide_multiply_fusion.1
  49.8 0.1 reshape.186
  49.9 0.8 broadcast_multiply_fusion.1
  50.7 3.1 %fusion.20 = f32[2,16,1,64]{3,2,1,0:T(1,128)S(1)} fusion(f32[2,16,128,1]{2,3,1,0:T(1,128)S(1)} %bitcast.277, f32[2,2,16,64,128]{4,3,2,1,0:T(8,128)} %param.38, f32[2,16,128]{2,1,0:T(8,128)S(1)} %bitcast.270, f32[2,16,64]{2,1,0:T(8,128)S(1)} %broadcast_multiply_fusion.1, f32[2,16]{1,0:T(2,128)} %fusion.2), kind=kOutput, calls=%fused_computation.24 | convolution fusion | flops 3932160 | bytes 1098752 | tf_op jit(solution)/shard_map/shpn,shn->shp/dot_general | solution.py:119
  53.8 0.8 multiply_reduce_fusion.2
  54.6 0.1 reduce_sum.52
  54.7 0.1 reduce_sum.53
  54.9 0.1 reshape.189
  55.0 5.2 %all-gather = bf16[4,2,1024]{2,1,0:T(2,128)(2,1)S(1)} all-gather(bf16[1,2,1024]{2,1,0:T(2,128)(2,1)S(1)} %fusion.72), channel_id=1, replica_groups=mesh['grp'=2,'tp'=4,'dp'=4] {'dp'}, dimensions={0}, use_global_device_ids=true | all-gather | bytes 20480 | tf_op jit(solution)/shard_map/all_gather | solution.py:133
  60.2 1.5 fusion.13
  61.7 18.7 %all-reduce.2 = f32[8,512]{1,0:T(8,128)S(1)} all-reduce(f32[8,512]{1,0:T(8,128)S(1)} %fusion.13), channel_id=4, replica_groups=mesh['grp'=2,'tp'=4,'dp'=4] {'tp'}, use_global_device_ids=true, to_apply=%region_6.7.clone | all-reduce | flops 4096 | bytes 32768
  80.4 11.9 %all-gather.1 = bf16[4,2,512]{2,1,0:T(2,128)(2,1)S(1)} all-gather(bf16[1,2,512]{2,1,0:T(2,128)(2,1)S(1)} %fusion.100), channel_id=1, replica_groups=mesh['grp'=2,'tp'=4,'dp'=4] {'tp'}, dimensions={0}, use_global_device_ids=true | all-gather | bytes 10240 | tf_op jit(solution)/shard_map/all_gather | solution.py:137
  92.4 0.1 multiply_convert_fusion
  92.5 0.1 fusion.50
  92.6 0.2 fusion.32
  92.8 1.4 fusion.34
  94.2 0.3 fusion.6
  94.5 0.3 fusion.8
  94.7 5.9 %all-reduce.6 = (f32[8]{0:T(128)S(1)}, f32[8,64]{1,0:T(8,128)S(1)}) all-reduce(f32[8]{0:T(128)S(1)} %get-tuple-element.28, f32[8,64]{1,0:T(8,128)S(1)} %fusion.50), channel_id=1, replica_groups=mesh['grp'=2,'tp'=4,'dp'=4] {'dp'}, use_global_device_ids=true, to_apply=%region_9.10 | all-reduce | flops 520 | bytes 4160 | tf_op jit(solution)/shard_map/psum | solution.py:82
  100.7 0.1 add_rsqrt_fusion.2
  100.8 0.7 pad_maximum_fusion.2
  101.5 0.1 compare_select_fusion
  101.6 0.9 fusion.3
  102.5 28.3 %all-reduce.13.cloned.1.call-done = f32[8,3072]{1,0:T(8,128)} async-done(((f32[8,3072]{1,0:T(8,128)}), f32[8,3072]{1,0:T(8,128)}) %all-reduce.13.cloned.1.call-update) | async-done | bytes 98320
  130.9 1.0 fusion.105
  131.9 0.1 divide_multiply_fusion.3
  132.0 0.1 divide_multiply_fusion
  132.1 0.1 reshape.190
  132.4 2.2 %multiply_add_fusion.1 = (f32[1,2,16,64,128]{4,3,2,1,0:T(8,128)S(1)}, f32[1,2,16,64,128]{4,3,2,1,0:T(8,128)S(1)}) fusion(f32[2,2,16,64,128]{4,3,2,1,0:T(8,128)} %param.38, f32[2,16,128]{2,1,0:T(8,128)S(1)} %bitcast.271, f32[2,16,64]{2,1,0:T(8,128)S(1)} %broadcast_multiply_fusion.1, f32[2,16]{1,0:T(2,128)S(1)} %copy-done.19, f32[2,16,128]{2,1,0:T(8,128)S(1)} %bitcast.272, ...), kind=kLoop, calls=%fused_computation.26 | loop fusion | flops 1572864 | bytes 4243712 | tf_op jit(solution)/shard_map/add | solution.py:116
  134.6 1.9 %fusion.11 = f32[2,16,1,64]{3,2,1,0:T(1,128)S(1)} fusion(f32[2,16,128,1]{2,3,1,0:T(1,128)S(1)} %bitcast.276, f32[2,2,16,64,128]{4,3,2,1,0:T(8,128)S(1)} %copy-done.2, f32[2,16,128]{2,1,0:T(8,128)S(1)} %bitcast.273, f32[2,16,64]{2,1,0:T(8,128)S(1)} %broadcast_multiply_fusion, f32[2,16]{1,0:T(2,128)S(1)} %fusion.3), kind=kOutput, calls=%fused_computation.15 | convolution fusion | flops 3932160 | bytes 1106944 | tf_op jit(solution)/shard_map/shpn,shn->shp/dot_general | solution.py:119
  136.5 0.2 multiply_reduce_fusion
  136.6 0.1 reduce_sum.56
  136.7 0.1 reduce_sum.57
  136.9 0.1 reshape.193
  137.0 5.2 %all-gather.2 = bf16[4,2,1024]{2,1,0:T(2,128)(2,1)S(1)} all-gather(bf16[1,2,1024]{2,1,0:T(2,128)(2,1)S(1)} %fusion.73), channel_id=1, replica_groups=mesh['grp'=2,'tp'=4,'dp'=4] {'dp'}, dimensions={0}, use_global_device_ids=true | all-gather | bytes 20480 | tf_op jit(solution)/shard_map/all_gather | solution.py:133
  142.2 1.5 fusion.4
  143.7 18.7 %all-reduce.5 = f32[8,512]{1,0:T(8,128)S(1)} all-reduce(f32[8,512]{1,0:T(8,128)S(1)} %fusion.4), channel_id=7, replica_groups=mesh['grp'=2,'tp'=4,'dp'=4] {'tp'}, use_global_device_ids=true, to_apply=%region_13.14.clone | all-reduce | flops 4096 | bytes 32768
  162.4 11.9 %all-gather.3 = bf16[4,2,512]{2,1,0:T(2,128)(2,1)S(1)} all-gather(bf16[1,2,512]{2,1,0:T(2,128)(2,1)S(1)} %fusion.101), channel_id=1, replica_groups=mesh['grp'=2,'tp'=4,'dp'=4] {'tp'}, dimensions={0}, use_global_device_ids=true | all-gather | bytes 10240 | tf_op jit(solution)/shard_map/all_gather | solution.py:137
  174.4 0.6 reshape.219
  175.0 0.6 pad_maximum_fusion.5
  175.6 0.6 pad_maximum_fusion.3
  176.3 0.6 pad_maximum_fusion.4
  176.9 1.5 pad_maximum_fusion
  (115 shorter events, 1.1 us)
Async XLA Ops:
  7.2 6.3 %copy-start.25 = (u32[32]{0:T(128)S(1)}, u32[32]{0:T(128)}, u32[]{:S(2)}) copy-start(u32[32]{0:T(128)} %constant.58) | copy-start | bytes 388
  7.2 5.1 %copy-start.4 = (bf16[8,512]{1,0:T(8,128)(2,1)S(1)}, bf16[8,512]{1,0:T(8,128)(2,1)}, u32[]{:S(2)}) copy-start(bf16[8,512]{1,0:T(8,128)(2,1)} %param.21) | copy-start | bytes 24580
  7.2 5.1 %copy-start = (bf16[2,512,1024]{2,1,0:T(8,128)(2,1)S(1)}, bf16[2,512,1024]{2,1,0:T(8,128)(2,1)}, u32[]{:S(2)}) copy-start(bf16[2,512,1024]{2,1,0:T(8,128)(2,1)} %param.25) | copy-start | bytes 6291460
  7.2 6.2 %copy-start.21 = (s32[2]{0:T(128)S(1)}, s32[2]{0:T(128)}, u32[]{:S(2)}) copy-start(s32[2]{0:T(128)} %param.22) | copy-start | bytes 28
  7.2 7.5 %copy-start.16 = (f32[2,16]{1,0:T(2,128)S(1)}, f32[2,16]{1,0:T(2,128)}, u32[]{:S(2)}) copy-start(f32[2,16]{1,0:T(2,128)} %param.29) | copy-start | bytes 388
  7.2 8.0 %copy-start.17 = (f32[2,16]{1,0:T(2,128)S(1)}, f32[2,16]{1,0:T(2,128)}, u32[]{:S(2)}) copy-start(f32[2,16]{1,0:T(2,128)} %param.30) | copy-start | bytes 388
  7.2 8.6 %copy-start.5 = (bf16[2,512,64]{1,2,0:T(8,128)(2,1)S(1)}, bf16[2,512,64]{1,2,0:T(8,128)(2,1)}, u32[]{:S(2)}) copy-start(bf16[2,512,64]{1,2,0:T(8,128)(2,1)} %param.28) | copy-start | bytes 393220
  7.2 8.7 %copy-start.12 = (f32[2,1024]{1,0:T(2,128)S(1)}, f32[2,1024]{1,0:T(2,128)}, u32[]{:S(2)}) copy-start(f32[2,1024]{1,0:T(2,128)} %param.36) | copy-start | bytes 24580
  7.3 8.7 %copy-start.10 = (bf16[2,4,512]{2,1,0:T(4,128)(2,1)S(1)}, bf16[2,4,512]{2,1,0:T(4,128)(2,1)}, u32[]{:S(2)}) copy-start(bf16[2,4,512]{2,1,0:T(4,128)(2,1)} %param.33) | copy-start | bytes 24580
  7.3 8.7 %copy-start.11 = (bf16[2,4,512]{2,1,0:T(4,128)(2,1)S(1)}, bf16[2,4,512]{2,1,0:T(4,128)(2,1)}, u32[]{:S(2)}) copy-start(bf16[2,4,512]{2,1,0:T(4,128)(2,1)} %param.34) | copy-start | bytes 24580
  7.3 8.7 %copy-start.6 = (bf16[2,2,3,1024]{3,1,2,0:T(2,128)(2,1)S(1)}, bf16[2,2,3,1024]{3,1,2,0:T(2,128)(2,1)}, u32[]{:S(2)}) copy-start(bf16[2,2,3,1024]{3,1,2,0:T(2,128)(2,1)} %param.39) | copy-start | bytes 73732
  7.3 8.7 %copy-start.7 = (bf16[2,4,1024]{2,1,0:T(4,128)(2,1)S(1)}, bf16[2,4,1024]{2,1,0:T(4,128)(2,1)}, u32[]{:S(2)}) copy-start(bf16[2,4,1024]{2,1,0:T(4,128)(2,1)} %param.32) | copy-start | bytes 49156
  7.3 18.0 %copy-start.8 = (bf16[2,2,3,512]{3,1,2,0:T(2,128)(2,1)S(1)}, bf16[2,2,3,512]{3,1,2,0:T(2,128)(2,1)}, u32[]{:S(2)}) copy-start(bf16[2,2,3,512]{3,1,2,0:T(2,128)(2,1)} %param.41) | copy-start | bytes 36868
  7.3 18.0 %copy-start.9 = (bf16[2,2,3,512]{3,1,2,0:T(2,128)(2,1)S(1)}, bf16[2,2,3,512]{3,1,2,0:T(2,128)(2,1)}, u32[]{:S(2)}) copy-start(bf16[2,2,3,512]{3,1,2,0:T(2,128)(2,1)} %param.40) | copy-start | bytes 36868
  7.3 40.5 %all-reduce.11.cloned.1.call-start = ((), (), s32[]{:S(2)}) async-start(), calls=%async_computation | async-start | bytes 196608
  8.2 18.8 %copy-start.18 = (f32[2,16]{1,0:T(2,128)S(1)}, f32[2,16]{1,0:T(2,128)}, u32[]{:S(2)}) copy-start(f32[2,16]{1,0:T(2,128)} %param.31) | copy-start | bytes 388
  8.2 19.4 %copy-start.24 = (u32[32]{0:T(128)S(1)}, u32[32]{0:T(128)}, u32[]{:S(2)}) copy-start(u32[32]{0:T(128)} %constant.66) | copy-start | bytes 388
  12.5 80.1 %copy-start.3 = (bf16[2,512,512]{2,1,0:T(8,128)(2,1)S(1)}, bf16[2,512,512]{2,1,0:T(8,128)(2,1)}, u32[]{:S(2)}) copy-start(bf16[2,512,512]{2,1,0:T(8,128)(2,1)} %param.27) | copy-start | bytes 3145732
  13.2 117.7 %all-reduce.13.cloned.1.call-start = ((), (), s32[]{:S(2)}) async-start(), calls=%async_computation.1 | async-start | bytes 196608
  13.4 14.2 %copy-start.26 = (f32[2]{0:T(128)}, f32[2]{0:T(128)S(1)}, u32[]{:S(2)}) copy-start(f32[2]{0:T(128)S(1)} %compare_convert_fusion) | copy-start | bytes 28
  13.4 14.2 %copy-start.22 = (s32[2]{0:T(128)}, s32[2]{0:T(128)S(1)}, u32[]{:S(2)}) copy-start(s32[2]{0:T(128)S(1)} %get-tuple-element.78) | copy-start | bytes 28
  25.5 3.4 %copy-start.13 = (f32[2,16]{1,0:T(2,128)}, f32[2,16]{1,0:T(2,128)S(1)}, u32[]{:S(2)}) copy-start(f32[2,16]{1,0:T(2,128)S(1)} %compare_select_fusion.1) | copy-start | bytes 388
  61.7 39.8 %copy-start.15 = (f32[16]{0:T(128)S(1)}, f32[16]{0:T(128)}, u32[]{:S(2)}) copy-start(f32[16]{0:T(128)} %get-tuple-element.76) | copy-start | bytes 196
  61.7 39.9 %copy-start.20 = (f32[16]{0:T(128)S(1)}, f32[16]{0:T(128)}, u32[]{:S(2)}) copy-start(f32[16]{0:T(128)} %get-tuple-element.74) | copy-start | bytes 196
  61.7 39.9 %copy-start.23 = (s32[2]{0:T(128)S(1)}, s32[2]{0:T(128)}, u32[]{:S(2)}) copy-start(s32[2]{0:T(128)} %copy-done.22) | copy-start | bytes 28
  61.7 39.9 %copy-start.27 = (f32[2]{0:T(128)S(1)}, f32[2]{0:T(128)}, u32[]{:S(2)}) copy-start(f32[2]{0:T(128)} %copy-done.26) | copy-start | bytes 28
  92.4 2.1 %copy-start.1 = (bf16[2,512,1024]{2,1,0:T(8,128)(2,1)S(1)}, bf16[2,512,1024]{2,1,0:T(8,128)(2,1)}, u32[]{:S(2)}) copy-start(bf16[2,512,1024]{2,1,0:T(8,128)(2,1)} %param.24) | copy-start | bytes 6291460
  92.5 39.9 %copy-start.19 = (f32[2,16]{1,0:T(2,128)S(1)}, f32[2,16]{1,0:T(2,128)}, u32[]{:S(2)}) copy-start(f32[2,16]{1,0:T(2,128)} %fusion.2) | copy-start | bytes 388
  132.4 2.2 %copy-start.2 = (f32[2,2,16,64,128]{4,3,2,1,0:T(8,128)S(1)}, f32[2,2,16,64,128]{4,3,2,1,0:T(8,128)}, u32[]{:S(2)}) copy-start(f32[2,2,16,64,128]{4,3,2,1,0:T(8,128)} %param.38) | copy-start | bytes 6291460
  132.4 4.1 %copy-start.14 = (f32[16]{0:T(128)S(1)}, f32[16]{0:T(128)}, u32[]{:S(2)}) copy-start(f32[16]{0:T(128)} %get-tuple-element.72) | copy-start | bytes 196
Sparse Core Ops, SparseCore 0:
  13.3 34.4 all-reduce.10
  101.6 29.2 all-reduce.12
where the time goes:
time: 186 us; the launch traced here: 185 us
  blocking collectives  86.2 us (46%)
  waiting for transfers between devices  47.3 us (25%)
  matrix products  16.9 us (9%)
  between operations  15.9 us (9%)
  other arithmetic  13.2 us (7%)
  local copies, waits for them, and re-layouts  5.54 us (3%)
    unnamed x4, waiting for transfers between devices  47.3 us
    unnamed x2, blocking collectives  37.4 us
    all_gather x2, blocking collectives, on_device(): stream = lax.all_gather(new_share, 'tp', axis=0, tiled=True)  23.9 us
    psum x2, blocking collectives, on_device(): squares_all = lax.psum(squares, 'dp')  14.5 us
    all_gather x2, blocking collectives, on_device(): lax.all_gather(gated_rows, 'dp', axis=0, tiled=True)  10.4 us
    dot_general x8, matrix products, on_device(): jnp.dot(normed, weight[layer_index], preferred_element_type=jnp.float32)  6.41 us
    dot_general x2, matrix products, on_device(): jnp.einsum('shpn,shn->shp', updated, read_heads, precision=lax.Precision....  4.94 us
  transfers between devices with their start and end apart: 2, of which 2 were waited for; matrix products, arithmetic and copies ran while one was open for 4% of the time, Pallas kernels for 0%

commit v1 on v0

--- a/solution.py
+++ b/solution.py
@@ -134,7 +134,9 @@
         branch_share = lax.psum_scatter(partial_out, "tp", scatter_dimension=0, tiled=True)
         stream_share = lax.dynamic_slice_in_dim(stream_float, share_first, share_rows, 0)
         new_share = (stream_share + branch_share).astype(jnp.bfloat16)
-        stream = lax.all_gather(new_share, "tp", axis=0, tiled=True)
+        stream = jnp.concatenate(
+            lax.all_to_all(jnp.stack([new_share] * lax.axis_size("tp")), "tp", 0, 0), axis=0
+        )
         states.append(updated)
         values.append(value_buf)
         writes.append(write_buf)

time: 186 us -> 176 us (0.946)
  blocking collectives: 86.2 us -> 62.6 us
  waiting for transfers between devices: 47.3 us -> 54.7 us
  starting transfers between devices: 0.08 us -> 6.58 us
    all_gather x2 -> x0, blocking collectives: 23.9 us -> none  [on_device(): stream = lax.all_gather(new_share, 'tp', axis=0, tiled=True)]
    all_to_all x0 -> x2, waiting for transfers between devices: none -> 7.52 us  [on_device(): lax.all_to_all(jnp.stack([new_share] * lax.axis_size('tp')), 'tp', 0, 0)]
    all_to_all x0 -> x2, starting transfers between devices: none -> 6.5 us  [on_device(): lax.all_to_all(jnp.stack([new_share] * lax.axis_size('tp')), 'tp', 0, 0)]
  transfers between devices with their start and end apart: 2 -> 4, of which waited for: 2 -> 4; matrix products, arithmetic and copies ran while one was open for 4% -> 6% of each run, Pallas kernels for 0% -> 0%
where the time goes in v1:
time: 176 us; the launch traced here: 175 us
  blocking collectives  62.6 us (36%)
  waiting for transfers between devices  54.7 us (31%)
  matrix products  16.2 us (9%)
  between operations  15.9 us (9%)
  other arithmetic  12.4 us (7%)
  local copies, waits for them, and re-layouts  6.89 us (4%)
  starting transfers between devices  6.58 us (4%)
    unnamed x4, waiting for transfers between devices  47.2 us
    unnamed x2, blocking collectives  37.6 us
    psum x2, blocking collectives, on_device(): squares_all = lax.psum(squares, 'dp')  14.6 us
    all_gather x2, blocking collectives, on_device(): lax.all_gather(gated_rows, 'dp', axis=0, tiled=True)  10.4 us
    all_to_all x2, waiting for transfers between devices, on_device(): lax.all_to_all(jnp.stack([new_share] * lax.axis_size('tp')), 'tp', 0, 0)  7.52 us
    all_to_all x2, starting transfers between devices, on_device(): lax.all_to_all(jnp.stack([new_share] * lax.axis_size('tp')), 'tp', 0, 0)  6.5 us
    dot_general x8, matrix products, on_device(): jnp.dot(normed, weight[layer_index], preferred_element_type=jnp.float32)  6.46 us
    dot_general x2, matrix products, on_device(): jnp.einsum('shpn,shn->shp', updated, read_heads, precision=lax.Precision....  4.93 us
  transfers between devices with their start and end apart: 4, of which 4 were waited for; matrix products, arithmetic and copies ran while one was open for 6% of the time, Pallas kernels for 0%

profile of v1, /device:TPU:0, one launch (start us, length us, event | category | flops | bytes accessed | tf_op | source)
XLA Modules:
  0.0 175.3 jit_solution(7389809470750810611)
XLA Ops:
  7.4 0.8 fusion.112
  8.2 1.3 fusion.38
  9.5 1.2 fusion.36
  10.8 1.5 fusion.17
  12.3 0.2 fusion.15
  12.5 0.7 pad_maximum_fusion.1
  13.2 0.1 multiply_reduce_fusion.3
  13.3 0.5 compare_convert_fusion
  13.8 0.6 dynamic-slice
  15.1 0.5 slice_bitcast_fusion.31
  15.6 0.6 negate_bitcast_fusion
  16.2 0.1 fusion.52
  16.5 8.6 %all-reduce.7 = (f32[8]{0:T(128)S(1)}, f32[8,64]{1,0:T(8,128)S(1)}) all-reduce(f32[8]{0:T(128)S(1)} %multiply_reduce_fusion.3, f32[8,64]{1,0:T(8,128)S(1)} %fusion.52), channel_id=1, replica_groups=mesh['grp'=2,'tp'=4,'dp'=4] {'dp'}, use_global_device_ids=true, to_apply=%region_2.0 | all-reduce | flops 520 | bytes 4160 | tf_op jit(solution)/shard_map/psum | solution.py:82
  25.3 0.1 compare_select_fusion.1
  25.4 1.5 fusion.2
  26.9 0.5 slice_bitcast_fusion.30
  27.4 1.3 dynamic-slice.4
  29.4 18.4 %all-reduce.11.cloned.1.call-done = f32[8,3072]{1,0:T(8,128)} async-done(((f32[8,3072]{1,0:T(8,128)}), f32[8,3072]{1,0:T(8,128)}) %all-reduce.11.cloned.1.call-update) | async-done | bytes 98320
  47.7 1.0 fusion.104
  48.8 0.1 divide_multiply_fusion.5
  49.0 0.1 divide_multiply_fusion.1
  49.2 3.1 %fusion.20 = f32[2,16,1,64]{3,2,1,0:T(1,128)S(1)} fusion(f32[2,16,128,1]{2,3,1,0:T(1,128)S(1)} %bitcast.273, f32[2,2,16,64,128]{4,3,2,1,0:T(8,128)} %param.38, f32[2,16,128]{2,1,0:T(8,128)S(1)} %bitcast.266, f32[2,16,64]{2,1,0:T(8,128)S(1)} %broadcast_multiply_fusion.1, f32[2,16]{1,0:T(2,128)} %fusion.2), kind=kOutput, calls=%fused_computation.24 | convolution fusion | flops 3932160 | bytes 1098752 | tf_op jit(solution)/shard_map/shpn,shn->shp/dot_general | solution.py:119
  52.3 0.8 multiply_reduce_fusion.2
  53.1 0.1 reduce_sum.54
  53.2 0.1 reduce_sum.55
  53.4 0.1 reshape.230
  53.5 5.2 %all-gather = bf16[4,2,1024]{2,1,0:T(2,128)(2,1)S(1)} all-gather(bf16[1,2,1024]{2,1,0:T(2,128)(2,1)S(1)} %fusion.72), channel_id=1, replica_groups=mesh['grp'=2,'tp'=4,'dp'=4] {'dp'}, dimensions={0}, use_global_device_ids=true | all-gather | bytes 20480 | tf_op jit(solution)/shard_map/all_gather | solution.py:133
  58.7 1.5 fusion.13
  60.2 18.9 %all-reduce.2 = f32[8,512]{1,0:T(8,128)S(1)} all-reduce(f32[8,512]{1,0:T(8,128)S(1)} %fusion.13), channel_id=4, replica_groups=mesh['grp'=2,'tp'=4,'dp'=4] {'tp'}, use_global_device_ids=true, to_apply=%region_6.7.clone | all-reduce | flops 4096 | bytes 32768
  79.1 0.6 stack.46
  79.7 3.2 %all-to-all-start = ((bf16[4,2,512]{2,1,0:T(2,128)(2,1)}), bf16[4,2,512]{2,1,0:T(2,128)(2,1)S(1)}, u32[]{:S(2)}, u32[]{:S(2)}) async-start(bf16[4,2,512]{2,1,0:T(2,128)(2,1)} %stack.46), calls=%async_computation | async-start | bytes 16384 | tf_op jit(solution)/shard_map/all_to_all | solution.py:138
  83.1 5.4 %all-to-all-done = bf16[4,2,512]{2,1,0:T(2,128)(2,1)S(1)} async-done(((bf16[4,2,512]{2,1,0:T(2,128)(2,1)}), bf16[4,2,512]{2,1,0:T(2,128)(2,1)S(1)}, u32[]{:S(2)}, u32[]{:S(2)}) %all-to-all-start) | async-done | bytes 8224 | tf_op jit(solution)/shard_map/all_to_all | solution.py:138
  88.5 0.1 multiply_convert_fusion
  88.6 0.1 fusion.50
  88.8 0.2 fusion.32
  88.9 0.3 fusion.6
  89.2 1.5 fusion.8
  90.8 0.2 fusion.34
  91.0 6.0 %all-reduce.6 = (f32[8]{0:T(128)S(1)}, f32[8,64]{1,0:T(8,128)S(1)}) all-reduce(f32[8]{0:T(128)S(1)} %reduce_sum.57, f32[8,64]{1,0:T(8,128)S(1)} %fusion.50), channel_id=1, replica_groups=mesh['grp'=2,'tp'=4,'dp'=4] {'dp'}, use_global_device_ids=true, to_apply=%region_9.10 | all-reduce | flops 520 | bytes 4160 | tf_op jit(solution)/shard_map/psum | solution.py:82
  97.0 0.1 add_rsqrt_fusion.2
  97.0 0.7 pad_maximum_fusion.2
  97.7 0.1 compare_select_fusion
  97.9 0.2 fusion.3
  98.1 28.8 %all-reduce.13.cloned.1.call-done = f32[8,3072]{1,0:T(8,128)} async-done(((f32[8,3072]{1,0:T(8,128)}), f32[8,3072]{1,0:T(8,128)}) %all-reduce.13.cloned.1.call-update) | async-done | bytes 98320
  126.9 1.0 fusion.103
  127.9 0.1 divide_multiply_fusion.3
  128.0 0.1 divide_multiply_fusion
  128.4 2.2 %multiply_add_fusion.1 = (f32[1,2,16,64,128]{4,3,2,1,0:T(8,128)S(1)}, f32[1,2,16,64,128]{4,3,2,1,0:T(8,128)S(1)}) fusion(f32[2,2,16,64,128]{4,3,2,1,0:T(8,128)} %param.38, f32[2,16,128]{2,1,0:T(8,128)S(1)} %bitcast.267, f32[2,16,64]{2,1,0:T(8,128)S(1)} %broadcast_multiply_fusion.1, f32[2,16]{1,0:T(2,128)S(1)} %copy-done.17, f32[2,16,128]{2,1,0:T(8,128)S(1)} %bitcast.268, ...), kind=kLoop, calls=%fused_computation.26 | loop fusion | flops 1572864 | bytes 4243712 | tf_op jit(solution)/shard_map/add | solution.py:116
  130.6 1.9 %fusion.11 = f32[2,16,1,64]{3,2,1,0:T(1,128)S(1)} fusion(f32[2,16,128,1]{2,3,1,0:T(1,128)S(1)} %bitcast.272, f32[2,2,16,64,128]{4,3,2,1,0:T(8,128)S(1)} %copy-done.1, f32[2,16,128]{2,1,0:T(8,128)S(1)} %bitcast.269, f32[2,16,64]{2,1,0:T(8,128)S(1)} %broadcast_multiply_fusion, f32[2,16]{1,0:T(2,128)S(1)} %fusion.3), kind=kOutput, calls=%fused_computation.15 | convolution fusion | flops 3932160 | bytes 1106944 | tf_op jit(solution)/shard_map/shpn,shn->shp/dot_general | solution.py:119
  132.4 0.2 multiply_reduce_fusion
  132.6 0.1 reduce_sum.59
  132.7 0.1 reduce_sum.60
  132.9 0.1 reshape.234
  133.0 5.2 %all-gather.1 = bf16[4,2,1024]{2,1,0:T(2,128)(2,1)S(1)} all-gather(bf16[1,2,1024]{2,1,0:T(2,128)(2,1)S(1)} %fusion.73), channel_id=1, replica_groups=mesh['grp'=2,'tp'=4,'dp'=4] {'dp'}, dimensions={0}, use_global_device_ids=true | all-gather | bytes 20480 | tf_op jit(solution)/shard_map/all_gather | solution.py:133
  138.2 1.5 fusion.4
  139.7 18.7 %all-reduce.5 = f32[8,512]{1,0:T(8,128)S(1)} all-reduce(f32[8,512]{1,0:T(8,128)S(1)} %fusion.4), channel_id=7, replica_groups=mesh['grp'=2,'tp'=4,'dp'=4] {'tp'}, use_global_device_ids=true, to_apply=%region_13.14.clone | all-reduce | flops 4096 | bytes 32768
  158.4 0.6 stack.47
  159.0 3.2 %all-to-all-start.1 = ((bf16[4,2,512]{2,1,0:T(2,128)(2,1)}), bf16[4,2,512]{2,1,0:T(2,128)(2,1)S(1)}, u32[]{:S(2)}, u32[]{:S(2)}) async-start(bf16[4,2,512]{2,1,0:T(2,128)(2,1)} %stack.47), calls=%async_computation.1 | async-start | bytes 16384 | tf_op jit(solution)/shard_map/all_to_all | solution.py:138
  162.3 0.6 pad_maximum_fusion.5
  162.9 0.6 pad_maximum_fusion.3
  163.6 1.5 pad_maximum_fusion
  165.1 0.6 pad_maximum_fusion.4
  165.7 2.1 %all-to-all-done.1 = bf16[4,2,512]{2,1,0:T(2,128)(2,1)S(1)} async-done(((bf16[4,2,512]{2,1,0:T(2,128)(2,1)}), bf16[4,2,512]{2,1,0:T(2,128)(2,1)S(1)}, u32[]{:S(2)}, u32[]{:S(2)}) %all-to-all-start.1) | async-done | bytes 8224 | tf_op jit(solution)/shard_map/all_to_all | solution.py:138
  167.8 0.6 reshape.235
  (115 shorter events, 1.5 us)
Async XLA Ops:
  7.2 6.7 %copy-start.23 = (u32[32]{0:T(128)S(1)}, u32[32]{0:T(128)}, u32[]{:S(2)}) copy-start(u32[32]{0:T(128)} %constant.58) | copy-start | bytes 388
  7.2 5.1 %copy-start.4 = (bf16[8,512]{1,0:T(8,128)(2,1)S(1)}, bf16[8,512]{1,0:T(8,128)(2,1)}, u32[]{:S(2)}) copy-start(bf16[8,512]{1,0:T(8,128)(2,1)} %param.21) | copy-start | bytes 24580
  7.2 5.1 %copy-start = (bf16[2,512,1024]{2,1,0:T(8,128)(2,1)S(1)}, bf16[2,512,1024]{2,1,0:T(8,128)(2,1)}, u32[]{:S(2)}) copy-start(bf16[2,512,1024]{2,1,0:T(8,128)(2,1)} %param.25) | copy-start | bytes 6291460
  7.2 6.1 %copy-start.20 = (s32[2]{0:T(128)S(1)}, s32[2]{0:T(128)}, u32[]{:S(2)}) copy-start(s32[2]{0:T(128)} %param.22) | copy-start | bytes 28
  7.2 7.9 %copy-start.14 = (f32[2,16]{1,0:T(2,128)S(1)}, f32[2,16]{1,0:T(2,128)}, u32[]{:S(2)}) copy-start(f32[2,16]{1,0:T(2,128)} %param.29) | copy-start | bytes 388
  7.2 8.4 %copy-start.15 = (f32[2,16]{1,0:T(2,128)S(1)}, f32[2,16]{1,0:T(2,128)}, u32[]{:S(2)}) copy-start(f32[2,16]{1,0:T(2,128)} %param.30) | copy-start | bytes 388
  7.2 9.0 %copy-start.5 = (bf16[2,512,64]{1,2,0:T(8,128)(2,1)S(1)}, bf16[2,512,64]{1,2,0:T(8,128)(2,1)}, u32[]{:S(2)}) copy-start(bf16[2,512,64]{1,2,0:T(8,128)(2,1)} %param.28) | copy-start | bytes 393220
  7.2 9.1 %copy-start.12 = (f32[2,1024]{1,0:T(2,128)S(1)}, f32[2,1024]{1,0:T(2,128)}, u32[]{:S(2)}) copy-start(f32[2,1024]{1,0:T(2,128)} %param.36) | copy-start | bytes 24580
  7.3 9.1 %copy-start.10 = (bf16[2,4,512]{2,1,0:T(4,128)(2,1)S(1)}, bf16[2,4,512]{2,1,0:T(4,128)(2,1)}, u32[]{:S(2)}) copy-start(bf16[2,4,512]{2,1,0:T(4,128)(2,1)} %param.33) | copy-start | bytes 24580
  7.3 9.1 %copy-start.11 = (bf16[2,4,512]{2,1,0:T(4,128)(2,1)S(1)}, bf16[2,4,512]{2,1,0:T(4,128)(2,1)}, u32[]{:S(2)}) copy-start(bf16[2,4,512]{2,1,0:T(4,128)(2,1)} %param.34) | copy-start | bytes 24580
  7.3 9.1 %copy-start.6 = (bf16[2,2,3,1024]{3,1,2,0:T(2,128)(2,1)S(1)}, bf16[2,2,3,1024]{3,1,2,0:T(2,128)(2,1)}, u32[]{:S(2)}) copy-start(bf16[2,2,3,1024]{3,1,2,0:T(2,128)(2,1)} %param.39) | copy-start | bytes 73732
  7.3 9.2 %copy-start.7 = (bf16[2,4,1024]{2,1,0:T(4,128)(2,1)S(1)}, bf16[2,4,1024]{2,1,0:T(4,128)(2,1)}, u32[]{:S(2)}) copy-start(bf16[2,4,1024]{2,1,0:T(4,128)(2,1)} %param.32) | copy-start | bytes 49156
  7.3 17.9 %copy-start.8 = (bf16[2,2,3,512]{3,1,2,0:T(2,128)(2,1)S(1)}, bf16[2,2,3,512]{3,1,2,0:T(2,128)(2,1)}, u32[]{:S(2)}) copy-start(bf16[2,2,3,512]{3,1,2,0:T(2,128)(2,1)} %param.41) | copy-start | bytes 36868
  7.3 17.9 %copy-start.9 = (bf16[2,2,3,512]{3,1,2,0:T(2,128)(2,1)S(1)}, bf16[2,2,3,512]{3,1,2,0:T(2,128)(2,1)}, u32[]{:S(2)}) copy-start(bf16[2,2,3,512]{3,1,2,0:T(2,128)(2,1)} %param.40) | copy-start | bytes 36868
  7.3 40.4 %all-reduce.11.cloned.1.call-start = ((), (), s32[]{:S(2)}) async-start(), calls=%async_computation.2 | async-start | bytes 196608
  8.2 18.7 %copy-start.16 = (f32[2,16]{1,0:T(2,128)S(1)}, f32[2,16]{1,0:T(2,128)}, u32[]{:S(2)}) copy-start(f32[2,16]{1,0:T(2,128)} %param.31) | copy-start | bytes 388
  13.2 75.6 %copy-start.2 = (bf16[2,512,512]{2,1,0:T(8,128)(2,1)S(1)}, bf16[2,512,512]{2,1,0:T(8,128)(2,1)}, u32[]{:S(2)}) copy-start(bf16[2,512,512]{2,1,0:T(8,128)(2,1)} %param.27) | copy-start | bytes 3145732
  13.8 11.6 %copy-start.21 = (s32[2]{0:T(128)}, s32[2]{0:T(128)S(1)}, u32[]{:S(2)}) copy-start(s32[2]{0:T(128)S(1)} %get-tuple-element.78) | copy-start | bytes 28
  60.2 37.5 %copy-start.13 = (f32[16]{0:T(128)S(1)}, f32[16]{0:T(128)}, u32[]{:S(2)}) copy-start(f32[16]{0:T(128)} %get-tuple-element.76) | copy-start | bytes 196
  60.2 37.6 %copy-start.18 = (f32[16]{0:T(128)S(1)}, f32[16]{0:T(128)}, u32[]{:S(2)}) copy-start(f32[16]{0:T(128)} %get-tuple-element.74) | copy-start | bytes 196
  60.2 37.6 %copy-start.19 = (f32[2,256,16]{1,2,0:T(8,128)S(1)}, f32[2,256,16]{1,2,0:T(8,128)}, u32[]{:S(2)}) copy-start(f32[2,256,16]{1,2,0:T(8,128)} %param.35) | copy-start | bytes 98308
  60.2 37.6 %copy-start.22 = (s32[2]{0:T(128)S(1)}, s32[2]{0:T(128)}, u32[]{:S(2)}) copy-start(s32[2]{0:T(128)} %copy-done.21) | copy-start | bytes 28
  79.1 18.8 %copy-start.24 = (f32[2]{0:T(128)S(1)}, f32[2]{0:T(128)}, u32[]{:S(2)}) copy-start(f32[2]{0:T(128)} %compare_convert_fusion) | copy-start | bytes 28
  79.7 8.8 %all-to-all-start = ((bf16[4,2,512]{2,1,0:T(2,128)(2,1)}), bf16[4,2,512]{2,1,0:T(2,128)(2,1)S(1)}, u32[]{:S(2)}, u32[]{:S(2)}) async-start(bf16[4,2,512]{2,1,0:T(2,128)(2,1)} %stack.46), calls=%async_computation | async-start | bytes 16384 | tf_op jit(solution)/shard_map/all_to_all | solution.py:138
  83.0 43.9 %all-reduce.13.cloned.1.call-start = ((), (), s32[]{:S(2)}) async-start(), calls=%async_computation.3 | async-start | bytes 196608
  88.6 39.7 %copy-start.17 = (f32[2,16]{1,0:T(2,128)S(1)}, f32[2,16]{1,0:T(2,128)}, u32[]{:S(2)}) copy-start(f32[2,16]{1,0:T(2,128)} %fusion.2) | copy-start | bytes 388
  88.9 1.9 %copy-start.3 = (bf16[2,512,512]{2,1,0:T(8,128)(2,1)S(1)}, bf16[2,512,512]{2,1,0:T(8,128)(2,1)}, u32[]{:S(2)}) copy-start(bf16[2,512,512]{2,1,0:T(8,128)(2,1)} %param.26) | copy-start | bytes 3145732
  128.4 2.2 %copy-start.1 = (f32[2,2,16,64,128]{4,3,2,1,0:T(8,128)S(1)}, f32[2,2,16,64,128]{4,3,2,1,0:T(8,128)}, u32[]{:S(2)}) copy-start(f32[2,2,16,64,128]{4,3,2,1,0:T(8,128)} %param.38) | copy-start | bytes 6291460
  159.0 8.8 %all-to-all-start.1 = ((bf16[4,2,512]{2,1,0:T(2,128)(2,1)}), bf16[4,2,512]{2,1,0:T(2,128)(2,1)S(1)}, u32[]{:S(2)}, u32[]{:S(2)}) async-start(bf16[4,2,512]{2,1,0:T(2,128)(2,1)} %stack.47), calls=%async_computation.1 | async-start | bytes 16384 | tf_op jit(solution)/shard_map/all_to_all | solution.py:138
Sparse Core Ops, SparseCore 0:
  13.3 34.3 all-reduce.10
  97.8 28.9 all-reduce.12
